TPU v7x, 32 devices: a whole 2x2x4 slice. The times are simulated.
32 devices in a mesh: sp: 8 (over z, x), tp: 4 (over y, core).
Axes of the slice: x: 2, y: 2, z: 4, core: 2. Of those that a mesh axis runs over, the one named last changes fastest.
Arguments:
- tokens: bfloat16 [768, 1024], P(('sp', 'tp')), may hold values from -11 to 11, as said below
- doc_ids: int32 [768], P('sp'), may hold values from 0 to 1, never falling along the last dimension, each value on 1 to 576 neighbouring positions
- query_down: bfloat16 [1024, 384], P('sp'), may hold values from -0.1875 to 0.1875
- query_gain: float32 [384], replicated, may hold values from 0.1 to 1.9
- query_up: bfloat16 [384, 16, 96], P('sp', 'tp'), may hold values from -0.3125 to 0.3125
- latent_down: bfloat16 [1024, 256], P('sp'), may hold values from -0.1875 to 0.1875
- latent_gain: float32 [256], replicated, may hold values from 0.1 to 1.9
- rope_down: bfloat16 [1024, 32], P('sp'), may hold values from -0.1875 to 0.1875
- key_up: bfloat16 [256, 16, 64], P('sp', 'tp'), may hold values from -0.375 to 0.375
- value_up: bfloat16 [256, 16, 64], P('sp', 'tp'), may hold values from -0.375 to 0.375
- output_weight: bfloat16 [1024, 1024], P('tp', 'sp'), may hold values from -0.1875 to 0.1875
- output_gain: float32 [1024], replicated, may hold values from 0.1 to 1.9
Outputs:
- layer_out: bfloat16 [768, 1024], P(('sp', 'tp'))
Inputs may be any that keep to these rules, and one draw needn't show every extreme that they name: Every entry of tokens lies between -11 and 11. `doc_ids`: document numbers never fall along the sequence; each document holds 1 to 576 positions.
All inputs are finite; a program needn't handle non-finite values.
Results may differ from a plain program's by a relative error of at most 0.02.
Values may be sent and summed in bfloat16 or wider, within the bound.
A program may use at most 64 MiB of HBM per device.

v0:
```python
import jax
import jax.numpy as jnp
from jax import lax
from jax.sharding import PartitionSpec as P

ROPE_BASE = 10000.0
EPS = 1e-06
MASKED = -1e30


def folded(value, axis, dim, update, carry):
    whole = jax.tree.map(lambda part: lax.all_gather(part, axis, axis=dim, tiled=True), value)
    return update(carry, whole, jnp.int32(0))


def gathered_then(share, axis, dim, apply):
    everything = lax.all_gather(share, axis, axis=dim, tiled=True)
    return apply(everything, jnp.int32(0))


def for_sending(value):

    def short(part):
        return part.astype(jnp.bfloat16) if part.dtype == jnp.float32 else part

    return jax.tree.map(short, value)


def own_rows(term, extent, axis):
    whole = term(jnp.int32(0), extent * lax.axis_size(axis)).astype(jnp.bfloat16)
    return lax.psum_scatter(whole, axis, scatter_dimension=0, tiled=True).astype(jnp.float32)


def normalize(values, gain_vec):
    return values * lax.rsqrt(jnp.mean(values * values, axis=-1, keepdims=True) + EPS) * gain_vec


def rotate(rope_part, position):
    half_width = rope_part.shape[-1] // 2
    frequency = ROPE_BASE ** (
        -jnp.arange(0, 2 * half_width, 2, dtype=jnp.float32) / (2 * half_width)
    )
    angles = position.astype(jnp.float32)[:, None] * frequency[None, :]
    cosine = jnp.cos(angles)
    sine_part = jnp.sin(angles)
    if rope_part.ndim == 3:
        cosine = cosine[:, None, :]
        sine_part = sine_part[:, None, :]
    first_half = rope_part[..., :half_width]
    second_half = rope_part[..., half_width:]
    return jnp.concatenate(
        [
            first_half * cosine - second_half * sine_part,
            first_half * sine_part + second_half * cosine,
        ],
        axis=-1,
    )


def on_device(
    tokens,
    doc_ids,
    query_down,
    query_gain,
    query_up,
    latent_down,
    latent_gain,
    rope_down,
    key_up,
    value_up,
    output_weight,
    output_gain,
):
    row_count = tokens.shape[0]
    key_span = doc_ids.shape[0]
    query_width = query_down.shape[1]
    latent_width = latent_down.shape[1]
    rope_width = rope_down.shape[1]
    local_heads = query_up.shape[1]
    head_width = query_up.shape[2]
    nope_width = key_up.shape[2]
    value_width = value_up.shape[2]

    def down_term(total_now, weight_rows, first_row):
        columns = lax.dynamic_slice_in_dim(tokens, first_row, weight_rows.shape[0], 1)
        return total_now + jnp.dot(columns, weight_rows, preferred_element_type=jnp.float32)

    empty_query = jnp.zeros((row_count, query_width), jnp.float32)
    empty_latent = jnp.zeros((row_count, latent_width), jnp.float32)
    empty_rope = jnp.zeros((row_count, rope_width), jnp.float32)
    query_sum = folded(query_down, "sp", 0, down_term, empty_query)
    latent_sum = folded(latent_down, "sp", 0, down_term, empty_latent)
    rope_sum = folded(rope_down, "sp", 0, down_term, empty_rope)
    query_lat = normalize(query_sum, query_gain).astype(jnp.bfloat16)
    kv_lat = normalize(latent_sum, latent_gain).astype(jnp.bfloat16)
    own_position = lax.axis_index(("sp", "tp")) * row_count + lax.iota(jnp.int32, row_count)
    rope_keys = rotate(rope_sum, own_position).astype(jnp.bfloat16)
    query_full, key_full, value_full = (
        lax.all_gather(query_up, "sp", axis=0, tiled=True),
        lax.all_gather(key_up, "sp", axis=0, tiled=True),
        lax.all_gather(value_up, "sp", axis=0, tiled=True),
    )
    flat_width = local_heads * head_width
    query_matrix = query_full.reshape(query_width, flat_width)
    block_offset = lax.axis_index("sp") * key_span

    def project(latent_rows, first_row):
        piece_rows = latent_rows.shape[0]
        raw_query = jnp.dot(
            latent_rows[:, :query_width], query_matrix, preferred_element_type=jnp.float32
        ).reshape(piece_rows, local_heads, head_width)
        position = block_offset + first_row + lax.iota(jnp.int32, piece_rows)
        turned = jnp.concatenate(
            [raw_query[..., :nope_width], rotate(raw_query[..., nope_width:], position)], axis=-1
        )
        return jnp.concatenate(
            [
                turned.astype(jnp.bfloat16).reshape(piece_rows, flat_width),
                latent_rows[:, query_width:],
            ],
            axis=1,
        )

    packed = jnp.concatenate([query_lat, kv_lat, rope_keys], axis=1)
    gathered = gathered_then(packed, "tp", 0, project)
    queries = gathered[:, :flat_width].reshape(key_span, local_heads, head_width)
    my_ids = doc_ids.astype(jnp.bfloat16)
    key_rows = jnp.concatenate([gathered[:, flat_width:], my_ids[:, None]], axis=1)
    query_nope = queries[..., :nope_width]
    query_rope = queries[..., nope_width:]
    score_scale = head_width ** (-0.5)
    absorbed = jnp.einsum("qhe,rhe->qhr", query_nope, key_full, preferred_element_type=jnp.float32)

    def block_scores(latent_part, rope_part):
        latent_float = latent_part.astype(jnp.float32)
        scores = jnp.einsum("qhr,kr->qhk", absorbed, latent_float, precision=lax.Precision.HIGHEST)
        scores = scores + jnp.einsum(
            "qhe,ke->qhk", query_rope, rope_part, preferred_element_type=jnp.float32
        )
        return (scores * score_scale, latent_float)

    def finish(averaged):
        return jnp.einsum(
            "qhr,rhv->qhv",
            averaged,
            value_full.astype(jnp.float32),
            precision=lax.Precision.HIGHEST,
        )

    def scan_step(state_now, block_keys):
        row_peak, row_total, running = state_now
        latent_part = block_keys[:, :latent_width]
        rope_part = block_keys[:, latent_width : latent_width + rope_width]
        block_ids = block_keys[:, latent_width + rope_width]
        scores, value_part = block_scores(latent_part, rope_part)
        same_doc = my_ids[:, None, None] == block_ids[None, None, :]
        peak_new = jnp.maximum(row_peak, jnp.max(jnp.where(same_doc, scores, MASKED), axis=-1))
        soft_weights = jnp.where(same_doc, jnp.exp(scores - peak_new[..., None]), 0.0)
        factor = jnp.exp(row_peak - peak_new)
        if value_part.ndim == 3:
            contrib = jnp.einsum(
                "qhk,khv->qhv", soft_weights, value_part, precision=lax.Precision.HIGHEST
            )
        else:
            contrib = jnp.einsum(
                "qhk,kv->qhv", soft_weights, value_part, precision=lax.Precision.HIGHEST
            )
        next_state = (
            peak_new,
            row_total * factor + jnp.sum(soft_weights, axis=-1),
            running * factor[..., None] + contrib,
        )
        return (next_state, None)

    def fold_keys(state_now, key_piece, first_row):
        key_blocks = key_piece.reshape(key_piece.shape[0] // key_span, key_span, key_piece.shape[1])
        return lax.scan(scan_step, state_now, key_blocks)[0]

    start_state = (
        jnp.full((key_span, local_heads), MASKED, jnp.float32),
        jnp.zeros((key_span, local_heads), jnp.float32),
        jnp.zeros((key_span, local_heads, latent_width), jnp.float32),
    )
    row_peak, row_total, running = folded(for_sending(key_rows), "sp", 0, fold_keys, start_state)
    averaged = running / row_total[..., None]
    attended = finish(averaged).astype(jnp.bfloat16).reshape(key_span, local_heads * value_width)
    out_full = lax.all_gather(output_weight, "sp", axis=1, tiled=True)

    def out_term(first_row, row_span):
        row_block = lax.dynamic_slice_in_dim(attended, first_row, row_span, 0)
        return jnp.dot(row_block, out_full, preferred_element_type=jnp.float32)

    mixed = own_rows(out_term, row_count, "tp")
    return normalize(mixed, output_gain).astype(jnp.bfloat16)


def solution(mesh):
    in_specs = (
        P(("sp", "tp"), None),
        P("sp"),
        P("sp", None),
        P(),
        P("sp", "tp", None),
        P("sp", None),
        P(),
        P("sp", None),
        P("sp", "tp", None),
        P("sp", "tp", None),
        P("tp", "sp"),
        P(),
    )
    out_specs = P(("sp", "tp"), None)
    return jax.shard_map(
        on_device, mesh=mesh, in_specs=in_specs, out_specs=out_specs, check_vma=False
    )
```

profile of v0, /device:TPU:0, one launch (start us, length us, event | category | flops | bytes accessed | tf_op | source)
XLA Modules:
  0.0 298.6 jit_solution(12510070031708650458)
XLA Ops:
  6.6 28.0 %all_gather.29 = bf16[1024,32]{0,1:T(8,128)(2,1)S(1)} all-gather(bf16[128,32]{0,1:T(8,128)(2,1)} %param.21), channel_id=1, replica_groups=mesh['sp'=8,'tp'=4] {'sp'}, dimensions={0}, use_global_device_ids=true | all-gather | bytes 73728 | tf_op jit(solution)/shard_map/all_gather | solution.py:12
  34.6 32.1 %all_gather.27 = bf16[1024,384]{1,0:T(8,128)(2,1)S(1)} all-gather(bf16[128,384]{1,0:T(8,128)(2,1)S(1)} %copy-done.3), channel_id=1, replica_groups=mesh['sp'=8,'tp'=4] {'sp'}, dimensions={0}, use_global_device_ids=true | all-gather | bytes 884736 | tf_op jit(solution)/shard_map/all_gather | solution.py:12
  67.1 0.5 copy-done.4
  67.6 31.3 %all_gather.28 = bf16[1024,256]{1,0:T(8,128)(2,1)S(1)} all-gather(bf16[128,256]{1,0:T(8,128)(2,1)S(1)} %copy-done.4), channel_id=1, replica_groups=mesh['sp'=8,'tp'=4] {'sp'}, dimensions={0}, use_global_device_ids=true | all-gather | bytes 589824 | tf_op jit(solution)/shard_map/all_gather | solution.py:12
  99.4 0.5 copy-done.10
  100.0 0.7 copy-done.11
  100.8 5.6 %all_gather.30 = bf16[96,672]{1,0:T(8,128)(2,1)S(1)} all-gather(bf16[24,672]{1,0:T(8,128)(2,1)S(1)} %pad_maximum_fusion.1), channel_id=1, replica_groups=mesh['sp'=8,'tp'=4] {'tp'}, dimensions={0}, use_global_device_ids=true | all-gather | bytes 161280 | tf_op jit(solution)/shard_map/all_gather | solution.py:17
  106.4 31.2 %all_gather.32 = bf16[384,4,96]{2,1,0:T(4,128)(2,1)S(1)} all-gather(bf16[48,4,96]{2,1,0:T(4,128)(2,1)S(1)} %copy-done.6), channel_id=1, replica_groups=mesh['sp'=8,'tp'=4] {'sp'}, dimensions={0}, use_global_device_ids=true | all-gather | bytes 331776 | tf_op jit(solution)/shard_map/all_gather | solution.py:99
  138.7 31.0 %all_gather.33 = bf16[256,4,64]{2,0,1:T(8,128)(2,1)S(1)} all-gather(bf16[32,4,64]{2,0,1:T(8,128)(2,1)S(1)} %copy.29), channel_id=1, replica_groups=mesh['sp'=8,'tp'=4] {'sp'}, dimensions={0}, use_global_device_ids=true | all-gather | bytes 147456 | tf_op jit(solution)/shard_map/all_gather | solution.py:100
  169.9 31.4 %all_gather.31 = bf16[768,289]{1,0:T(8,128)(2,1)S(1)} all-gather(bf16[96,289]{1,0:T(8,128)(2,1)S(1)} %pad_maximum_fusion), channel_id=1, replica_groups=mesh['sp'=8,'tp'=4] {'sp'}, dimensions={0}, use_global_device_ids=true | all-gather | bytes 499392 | tf_op jit(solution)/shard_map/all_gather | solution.py:12
  201.6 11.6 %while.15 = (s32[]{:T(128)}, f32[96,4]{0,1:T(4,128)S(1)}, f32[96,4]{0,1:T(4,128)S(1)}, f32[96,4,256]{2,0,1:T(8,128)S(1)}, bf16[96]{0:T(256)(128)(2,1)S(1)}, /*in...) while((s32[]{:T(128)}, f32[96,4]{0,1:T(4,128)S(1)}, ...), condition=%wide.region_5.6_spmd.clone, body=%wide.region_2.5_spmd.clone.sunk | while | flops 229489536 | bytes 2351349 | solution.py:177
  202.6 0.5 convolution_add_fusion.3
  204.0 0.5 convolution_add_fusion.3
  205.5 0.5 convolution_add_fusion.3
  206.9 0.5 convolution_add_fusion.3
  208.4 0.5 convolution_add_fusion.3
  209.8 0.5 convolution_add_fusion.3
  213.3 31.0 %all_gather.34 = bf16[256,4,64]{2,0,1:T(8,128)(2,1)S(1)} all-gather(bf16[32,4,64]{2,0,1:T(8,128)(2,1)S(1)} %copy.30), channel_id=1, replica_groups=mesh['sp'=8,'tp'=4] {'sp'}, dimensions={0}, use_global_device_ids=true | all-gather | bytes 147456 | tf_op jit(solution)/shard_map/all_gather | solution.py:101
  244.3 27.0 %all_gather.35 = bf16[256,1024]{1,0:T(8,128)(2,1)S(1)} all-gather(bf16[256,128]{1,0:T(8,128)(2,1)S(1)} %copy-done.5), channel_id=1, replica_groups=mesh['sp'=8,'tp'=4] {'sp'}, dimensions={1}, use_global_device_ids=true | all-gather | bytes 589824 | tf_op jit(solution)/shard_map/all_gather | solution.py:187
  271.3 0.5 convolution_convert_fusion.1
  271.8 0.9 convolution_convert_fusion
  272.8 17.3 %reduce-scatter.2.cloned.1.call-done = bf16[24,1024]{1,0:T(8,128)(2,1)} async-done(((bf16[96,1024]{1,0:T(8,128)(2,1)}), bf16[24,1024]{1,0:T(8,128)(2,1)}) %reduce-scatter.2.cloned.1.call-update) | async-done | bytes 49168 | tf_op jit(solution)/shard_map/reduce_scatter | solution.py:31
  290.1 1.0 fusion.13
  291.1 0.7 fusion.15
  (128 shorter events, 11.1 us)
Async XLA Ops:
  6.5 60.1 %copy-start = (bf16[24,1024]{1,0:T(8,128)(2,1)S(1)}, bf16[24,1024]{1,0:T(8,128)(2,1)}, u32[]{:S(2)}) copy-start(bf16[24,1024]{1,0:T(8,128)(2,1)} %param.14) | copy-start | bytes 147460
  6.5 28.1 %copy-start.3 = (bf16[128,384]{1,0:T(8,128)(2,1)S(1)}, bf16[128,384]{1,0:T(8,128)(2,1)}, u32[]{:S(2)}) copy-start(bf16[128,384]{1,0:T(8,128)(2,1)} %param.16) | copy-start | bytes 294916
  6.5 283.5 %reduce-scatter.2.cloned.1.call-start = ((), (), s32[]{:S(2)}) async-start(), calls=%async_computation.1 | async-start | bytes 245760 | tf_op jit(solution)/shard_map/reduce_scatter | solution.py:31
  66.8 0.9 copy-start.4
  99.2 0.7 copy-start.10
  100.0 0.7 copy-start.11
  100.8 5.6 %copy-start.6 = (bf16[48,4,96]{2,1,0:T(4,128)(2,1)S(1)}, bf16[48,4,96]{2,1,0:T(4,128)(2,1)}, u32[]{:S(2)}) copy-start(bf16[48,4,96]{2,1,0:T(4,128)(2,1)} %param.18) | copy-start | bytes 110596
  106.4 31.5 %copy-start.1 = (bf16[96,672]{1,0:T(8,128)(2,1)}, bf16[96,672]{1,0:T(8,128)(2,1)S(1)}, u32[]{:S(2)}) copy-start(bf16[96,672]{1,0:T(8,128)(2,1)S(1)} %all_gather.30) | copy-start | bytes 387076
  137.9 0.8 copy-start.7
  138.7 31.0 %copy-start.12 = (s32[96]{0:T(128)S(1)}, s32[96]{0:T(128)}, u32[]{:S(2)}) copy-start(s32[96]{0:T(128)} %param.15) | copy-start | bytes 1156
  138.7 31.2 %slice-start = ((bf16[96,672]{1,0:T(8,128)(2,1)}), bf16[96,288]{1,0:T(8,128)(2,1)S(1)}, s32[]{:S(2)}) async-start(bf16[96,672]{1,0:T(8,128)(2,1)} %copy-done.1), calls=%async_computation.2 | async-start | bytes 147456 | tf_op jit(solution)/shard_map/slice | solution.py:119
  201.6 11.6 %copy-start.8 = (bf16[32,4,64]{2,1,0:T(4,128)(2,1)S(1)}, bf16[32,4,64]{2,1,0:T(4,128)(2,1)}, u32[]{:S(2)}) copy-start(bf16[32,4,64]{2,1,0:T(4,128)(2,1)} %param.23) | copy-start | bytes 49156
  213.2 31.1 %copy-start.5 = (bf16[256,128]{1,0:T(8,128)(2,1)S(1)}, bf16[256,128]{1,0:T(8,128)(2,1)}, u32[]{:S(2)}) copy-start(bf16[256,128]{1,0:T(8,128)(2,1)} %param.24) | copy-start | bytes 196612
  272.7 18.3 %copy-start.9 = (f32[1024]{0:T(1024)S(1)}, f32[1024]{0:T(1024)}, u32[]{:S(2)}) copy-start(f32[1024]{0:T(1024)} %param.25) | copy-start | bytes 12292
  290.1 1.0 copy-start.2
Sparse Core Ops, SparseCore 0:
  272.9 17.1 reduce-scatter.1
where the time goes:
time: 299 us
  blocking collectives  249 us (83%)
  waiting for transfers between devices  17.3 us (6%)
  between operations  13.6 us (5%)
  matrix products  10.7 us (4%)
  local copies, waits for them, and re-layouts  4.08 us (1%)
  other arithmetic  3.78 us (1%)
    all_gather x4, blocking collectives, folded(): lax.all_gather(part, axis, axis=dim, tiled=True)  123 us
    all_gather x1, blocking collectives, on_device(): lax.all_gather(query_up, 'sp', axis=0, tiled=True)  31.2 us
    all_gather x1, blocking collectives, on_device(): lax.all_gather(value_up, 'sp', axis=0, tiled=True)  31 us
    all_gather x1, blocking collectives, on_device(): lax.all_gather(key_up, 'sp', axis=0, tiled=True)  31 us
    all_gather x1, blocking collectives, on_device(): out_full = lax.all_gather(output_weight, 'sp', axis=1, tiled=True)  27 us
    reduce_scatter x1, waiting for transfers between devices, own_rows(): lax.psum_scatter(whole, axis, scatter_dimension=0, tiled=True)  17.3 us
  transfers between devices with their start and end apart: 1, of which 1 were waited for; matrix products, arithmetic and copies ran while one was open for 0% of the time, Pallas kernels for 0%

commit v1 on v0

--- a/solution.py
+++ b/solution.py
@@ -6,6 +6,13 @@
 ROPE_BASE = 10000.0
 EPS = 1e-06
 MASKED = -1e30
+
+
+def all_by_exchange(value, name, dim):
+    peers = lax.axis_size(name)
+    blocks = jnp.stack([value for _ in range(peers)])
+    blocks = lax.all_to_all(blocks, name, split_axis=0, concat_axis=0)
+    return jnp.concatenate(blocks, axis=dim)
 
 
 def folded(value, axis, dim, update, carry):
@@ -98,7 +105,7 @@
     query_full, key_full, value_full = (
         lax.all_gather(query_up, "sp", axis=0, tiled=True),
         lax.all_gather(key_up, "sp", axis=0, tiled=True),
-        lax.all_gather(value_up, "sp", axis=0, tiled=True),
+        all_by_exchange(value_up, "sp", 0),
     )
     flat_width = local_heads * head_width
     query_matrix = query_full.reshape(query_width, flat_width)

time: 299 us -> 276 us (0.923)
  blocking collectives: 249 us -> 216 us
  starting transfers between devices: 0.01 us -> 7.45 us
    all_gather x1 -> x0, blocking collectives: 31 us -> none  [on_device(): lax.all_gather(value_up, 'sp', axis=0, tiled=True)]
    all_to_all x0 -> x1, starting transfers between devices: none -> 7.41 us  [all_by_exchange(): blocks = lax.all_to_all(blocks, name, split_axis=0, concat_axis=0)]
  transfers between devices with their start and end apart: 1 -> 2, of which waited for: 1 -> 1; matrix products, arithmetic and copies ran while one was open for 0% -> 5% of each run, Pallas kernels for 0% -> 0%
where the time goes in v1:
time: 276 us; the launch traced here: 275 us
  blocking collectives  216 us (78%)
  waiting for transfers between devices  17.5 us (6%)
  between operations  13.7 us (5%)
  matrix products  10.7 us (4%)
  starting transfers between devices  7.45 us (3%)
  local copies, waits for them, and re-layouts  5.69 us (2%)
  other arithmetic  3.79 us (1%)
    all_gather x4, blocking collectives, folded(): lax.all_gather(part, axis, axis=dim, tiled=True)  122 us
    all_gather x1, blocking collectives, on_device(): lax.all_gather(query_up, 'sp', axis=0, tiled=True)  31.1 us
    all_gather x1, blocking collectives, on_device(): lax.all_gather(key_up, 'sp', axis=0, tiled=True)  30.9 us
    all_gather x1, blocking collectives, on_device(): out_full = lax.all_gather(output_weight, 'sp', axis=1, tiled=True)  27 us
    reduce_scatter x1, waiting for transfers between devices, own_rows(): lax.psum_scatter(whole, axis, scatter_dimension=0, tiled=True)  17.5 us
    all_to_all x1, starting transfers between devices, all_by_exchange(): blocks = lax.all_to_all(blocks, name, split_axis=0, concat_axis=0)  7.41 us
    all_gather x1, blocking collectives, gathered_then(): everything = lax.all_gather(share, axis, axis=dim, tiled=True)  5.58 us
  transfers between devices with their start and end apart: 2, of which 1 were waited for; matrix products, arithmetic and copies ran while one was open for 5% of the time, Pallas kernels for 0%

profile of v1, /device:TPU:0, one launch (start us, length us, event | category | flops | bytes accessed | tf_op | source)
XLA Modules:
  0.0 275.5 jit_solution(7167321162988163040)
XLA Ops:
  6.5 0.8 copy.31
  7.4 0.9 reshape.149
  8.2 7.4 %all-to-all-start = ((bf16[8,2,4096]{2,1,0:T(2,128)(2,1)}), bf16[8,2,4096]{2,1,0:T(2,128)(2,1)S(1)}, u32[]{:S(2)}, u32[]{:S(2)}) async-start(bf16[8,2,4096]{2,1,0:T(2,128)(2,1)} %reshape.149), calls=%async_computation | async-start | bytes 262144 | tf_op jit(solution)/shard_map/all_to_all | solution.py:14
  15.8 26.5 %all_gather.26 = bf16[1024,32]{0,1:T(8,128)(2,1)S(1)} all-gather(bf16[128,32]{0,1:T(8,128)(2,1)S(1)} %copy-done.8), channel_id=1, replica_groups=mesh['sp'=8,'tp'=4] {'sp'}, dimensions={0}, use_global_device_ids=true | all-gather | bytes 73728 | tf_op jit(solution)/shard_map/all_gather | solution.py:19
  42.3 32.0 %all_gather.24 = bf16[1024,384]{1,0:T(8,128)(2,1)S(1)} all-gather(bf16[128,384]{1,0:T(8,128)(2,1)S(1)} %copy-done.3), channel_id=1, replica_groups=mesh['sp'=8,'tp'=4] {'sp'}, dimensions={0}, use_global_device_ids=true | all-gather | bytes 884736 | tf_op jit(solution)/shard_map/all_gather | solution.py:19
  74.8 0.5 copy-done.4
  75.3 31.3 %all_gather.25 = bf16[1024,256]{1,0:T(8,128)(2,1)S(1)} all-gather(bf16[128,256]{1,0:T(8,128)(2,1)S(1)} %copy-done.4), channel_id=1, replica_groups=mesh['sp'=8,'tp'=4] {'sp'}, dimensions={0}, use_global_device_ids=true | all-gather | bytes 589824 | tf_op jit(solution)/shard_map/all_gather | solution.py:19
  107.4 0.7 copy-done.11
  108.2 5.6 %all_gather.27 = bf16[96,672]{1,0:T(8,128)(2,1)S(1)} all-gather(bf16[24,672]{1,0:T(8,128)(2,1)S(1)} %pad_maximum_fusion.1), channel_id=1, replica_groups=mesh['sp'=8,'tp'=4] {'tp'}, dimensions={0}, use_global_device_ids=true | all-gather | bytes 161280 | tf_op jit(solution)/shard_map/all_gather | solution.py:24
  113.8 31.1 %all_gather.29 = bf16[384,4,96]{2,1,0:T(4,128)(2,1)S(1)} all-gather(bf16[48,4,96]{2,1,0:T(4,128)(2,1)S(1)} %copy-done.6), channel_id=1, replica_groups=mesh['sp'=8,'tp'=4] {'sp'}, dimensions={0}, use_global_device_ids=true | all-gather | bytes 331776 | tf_op jit(solution)/shard_map/all_gather | solution.py:106
  146.0 30.9 %all_gather.30 = bf16[256,4,64]{2,0,1:T(8,128)(2,1)S(1)} all-gather(bf16[32,4,64]{2,0,1:T(8,128)(2,1)S(1)} %copy.30), channel_id=1, replica_groups=mesh['sp'=8,'tp'=4] {'sp'}, dimensions={0}, use_global_device_ids=true | all-gather | bytes 147456 | tf_op jit(solution)/shard_map/all_gather | solution.py:107
  177.1 31.7 %all_gather.28 = bf16[768,289]{1,0:T(8,128)(2,1)S(1)} all-gather(bf16[96,289]{1,0:T(8,128)(2,1)S(1)} %pad_maximum_fusion), channel_id=1, replica_groups=mesh['sp'=8,'tp'=4] {'sp'}, dimensions={0}, use_global_device_ids=true | all-gather | bytes 499392 | tf_op jit(solution)/shard_map/all_gather | solution.py:19
  209.1 11.6 %while.15 = (s32[]{:T(128)}, f32[96,4]{0,1:T(4,128)S(1)}, f32[96,4]{0,1:T(4,128)S(1)}, f32[96,4,256]{2,0,1:T(8,128)S(1)}, bf16[96]{0:T(256)(128)(2,1)S(1)}, /*in...) while((s32[]{:T(128)}, f32[96,4]{0,1:T(4,128)S(1)}, ...), condition=%wide.region_5.6_spmd.clone, body=%wide.region_2.5_spmd.clone.sunk | while | flops 229489536 | bytes 2351349 | solution.py:184
  210.0 0.5 convolution_add_fusion.3
  211.5 0.5 convolution_add_fusion.3
  212.9 0.5 convolution_add_fusion.3
  214.4 0.5 convolution_add_fusion.3
  215.8 0.5 convolution_add_fusion.3
  220.7 27.0 %all_gather.31 = bf16[256,1024]{1,0:T(8,128)(2,1)S(1)} all-gather(bf16[256,128]{1,0:T(8,128)(2,1)S(1)} %copy-done.5), channel_id=1, replica_groups=mesh['sp'=8,'tp'=4] {'sp'}, dimensions={1}, use_global_device_ids=true | all-gather | bytes 589824 | tf_op jit(solution)/shard_map/all_gather | solution.py:194
  248.0 0.5 convolution_convert_fusion.1
  248.5 0.9 convolution_convert_fusion
  249.4 17.5 %reduce-scatter.2.cloned.1.call-done = bf16[24,1024]{1,0:T(8,128)(2,1)} async-done(((bf16[96,1024]{1,0:T(8,128)(2,1)}), bf16[24,1024]{1,0:T(8,128)(2,1)}) %reduce-scatter.2.cloned.1.call-update) | async-done | bytes 49168 | tf_op jit(solution)/shard_map/reduce_scatter | solution.py:38
  266.9 1.0 fusion.13
  267.9 0.7 fusion.15
  (133 shorter events, 12.1 us)
Async XLA Ops:
  6.5 67.8 %copy-start = (bf16[24,1024]{1,0:T(8,128)(2,1)S(1)}, bf16[24,1024]{1,0:T(8,128)(2,1)}, u32[]{:S(2)}) copy-start(bf16[24,1024]{1,0:T(8,128)(2,1)} %param.14) | copy-start | bytes 147460
  8.2 7.5 %copy-start.8 = (bf16[128,32]{0,1:T(8,128)(2,1)S(1)}, bf16[128,32]{0,1:T(8,128)(2,1)}, u32[]{:S(2)}) copy-start(bf16[128,32]{0,1:T(8,128)(2,1)} %param.21) | copy-start | bytes 24580
  8.2 239.5 %all-to-all-start = ((bf16[8,2,4096]{2,1,0:T(2,128)(2,1)}), bf16[8,2,4096]{2,1,0:T(2,128)(2,1)S(1)}, u32[]{:S(2)}, u32[]{:S(2)}) async-start(bf16[8,2,4096]{2,1,0:T(2,128)(2,1)} %reshape.149), calls=%async_computation | async-start | bytes 262144 | tf_op jit(solution)/shard_map/all_to_all | solution.py:14
  15.7 26.6 %copy-start.3 = (bf16[128,384]{1,0:T(8,128)(2,1)S(1)}, bf16[128,384]{1,0:T(8,128)(2,1)}, u32[]{:S(2)}) copy-start(bf16[128,384]{1,0:T(8,128)(2,1)} %param.16) | copy-start | bytes 294916
  15.7 251.3 %reduce-scatter.2.cloned.1.call-start = ((), (), s32[]{:S(2)}) async-start(), calls=%async_computation.2 | async-start | bytes 245760 | tf_op jit(solution)/shard_map/reduce_scatter | solution.py:38
  74.4 0.9 copy-start.4
  106.6 0.7 copy-start.10
  107.4 0.7 copy-start.11
  108.2 5.6 %copy-start.6 = (bf16[48,4,96]{2,1,0:T(4,128)(2,1)S(1)}, bf16[48,4,96]{2,1,0:T(4,128)(2,1)}, u32[]{:S(2)}) copy-start(bf16[48,4,96]{2,1,0:T(4,128)(2,1)} %param.18) | copy-start | bytes 110596
  113.8 31.4 %copy-start.1 = (bf16[96,672]{1,0:T(8,128)(2,1)}, bf16[96,672]{1,0:T(8,128)(2,1)S(1)}, u32[]{:S(2)}) copy-start(bf16[96,672]{1,0:T(8,128)(2,1)S(1)} %all_gather.27) | copy-start | bytes 387076
  145.2 0.8 copy-start.7
  146.0 30.9 %copy-start.12 = (s32[96]{0:T(128)S(1)}, s32[96]{0:T(128)}, u32[]{:S(2)}) copy-start(s32[96]{0:T(128)} %param.15) | copy-start | bytes 1156
  146.0 31.0 %slice-start = ((bf16[96,672]{1,0:T(8,128)(2,1)}), bf16[96,288]{1,0:T(8,128)(2,1)S(1)}, s32[]{:S(2)}) async-start(bf16[96,672]{1,0:T(8,128)(2,1)} %copy-done.1), calls=%async_computation.3 | async-start | bytes 147456 | tf_op jit(solution)/shard_map/slice | solution.py:126
  209.1 11.6 %copy-start.5 = (bf16[256,128]{1,0:T(8,128)(2,1)S(1)}, bf16[256,128]{1,0:T(8,128)(2,1)}, u32[]{:S(2)}) copy-start(bf16[256,128]{1,0:T(8,128)(2,1)} %param.24) | copy-start | bytes 196612
  248.5 19.5 %copy-start.9 = (f32[1024]{0:T(1024)S(1)}, f32[1024]{0:T(1024)}, u32[]{:S(2)}) copy-start(f32[1024]{0:T(1024)} %param.25) | copy-start | bytes 12292
  266.9 1.0 copy-start.2
Sparse Core Ops, SparseCore 0:
  249.5 17.3 reduce-scatter.1
